TPU v7x, 256 devices: a whole 4x4x8 slice. The times are simulated.
256 devices in a mesh: fs: 32 (over z, x), tp: 8 (over y, core).
Axes of the slice: x: 4, y: 4, z: 8, core: 2. Of those that a mesh axis runs over, the one named last changes fastest.
Arguments:
- tokens: bfloat16 [32768, 2048], P(('fs', 'tp')), may hold values from -6 to 6
- gate_pre: bfloat16 [32768, 5632], P('fs', 'tp'), may hold values from -6 to 6
- value_pre: bfloat16 [32768, 5632], P('fs', 'tp'), may hold values from -6 to 6
- up_gate_w: bfloat16 [2048, 5632], P('fs', 'tp'), may hold values from -0.078125 to 0.078125
- up_value_w: bfloat16 [2048, 5632], P('fs', 'tp'), may hold values from -0.078125 to 0.078125
- conv_weight: float32 [3, 5632], P(None, 'tp'), may hold values from -3 to 3
- conv_bias: float32 [5632], P('tp'), may hold values from -3 to 3
- hidden_grad: bfloat16 [32768, 5632], P('fs', 'tp'), may hold values from -6 to 6
Outputs:
- input_grad: bfloat16 [32768, 2048], P(('fs', 'tp'))
- up_gate_grad: float32 [2048, 5632], P('fs', 'tp')
- up_value_grad: float32 [2048, 5632], P('fs', 'tp')
- conv_weight_grad: float32 [3, 5632], P(None, 'tp')
- conv_bias_grad: float32 [5632], P('tp')
All inputs are finite; a program needn't handle non-finite values.
Results may differ from a plain program's by a relative error of at most 0.013.
Values may be sent and summed in bfloat16 or wider, within the bound.
No kernel may reach another device: no remote copies, remote signals or barrier semaphores. Data moves between devices by JAX's collectives and lax.ppermute only.
A program may use at most 128 MiB of HBM per device.

v0:
```python
import jax
import jax.numpy as jnp
from jax import lax
from jax.sharding import Mesh
from jax.sharding import PartitionSpec as P

FS = ("fs_0", "fs_1")
FS_TP = ("fs_0", "fs_1", "tp")


def copy_for_each(shard, axis):
    peers = lax.axis_size(axis)
    return lax.all_to_all(
        jnp.broadcast_to(shard[None], (peers, *shard.shape)), axis, 0, 0, tiled=True
    )


def taken_together(shard, axis):
    return copy_for_each(shard, axis).sum(axis=0)


def in_one_piece(arrays, axis, dim, along):
    ends, at = ([], 0)
    for a in arrays[:-1]:
        at += a.shape[along]
        ends.append(at)
    both = jnp.concatenate(arrays, axis=along)
    return tuple(jnp.split(lax.all_gather(both, axis, axis=dim, tiled=True), ends, axis=along))


def summed_rows(subtotal, axes):
    for axis in axes:
        subtotal = lax.psum_scatter(subtotal, axis, scatter_dimension=0, tiled=True)
    return subtotal


def in_blocks(shard, dim, peers):
    lengths = shard.shape
    blocks = shard.reshape(*lengths[:dim], peers, lengths[dim] // peers, *lengths[dim + 1 :])
    return jnp.moveaxis(blocks, dim, 0)


def summed_on_arrival(shard, axis, dim):
    blocks = in_blocks(shard, dim, lax.axis_size(axis))
    arrived = lax.all_to_all(blocks, axis, split_axis=0, concat_axis=0, tiled=True)
    return arrived.astype(jnp.float32).sum(axis=0)


def contract_rows(left, right):
    return lax.dot_general(
        left, right, (((0,), (0,)), ((), ())), preferred_element_type=jnp.float32
    )


def contract_cols(left, right):
    return lax.dot_general(
        left, right, (((1,), (1,)), ((), ())), preferred_element_type=jnp.float32
    )


def on_device(
    tokens, gate_pre, value_pre, up_gate_w, up_value_w, conv_weight, conv_bias, hidden_grad
):
    length = gate_pre.shape[0]
    col_count = gate_pre.shape[1]
    scale = float(length * lax.axis_size(FS)) ** (-0.5)
    gate_float = gate_pre.astype(jnp.float32)
    padded = jnp.pad(gate_float, ((2, 0), (0, 0)))
    gate_conv = (
        conv_bias
        + conv_weight[0] * padded[:length]
        + conv_weight[1] * padded[1 : length + 1]
        + conv_weight[2] * padded[2:]
    )
    active, gelu_back = jax.vjp(jax.nn.gelu, gate_conv)
    grad_float = hidden_grad.astype(jnp.float32)
    value_grad = (grad_float * active).astype(jnp.bfloat16)
    conv_grad = gelu_back(grad_float * value_pre.astype(jnp.float32))[0]
    shifted = jnp.pad(conv_grad, ((0, 2), (0, 0)))
    gate_grad = (
        conv_weight[2] * conv_grad
        + conv_weight[1] * shifted[1 : length + 1]
        + conv_weight[0] * shifted[2:]
    ).astype(jnp.bfloat16)
    conv_terms = jnp.stack(
        [
            jnp.sum(conv_grad * padded[:length], axis=0),
            jnp.sum(conv_grad * padded[1 : length + 1], axis=0),
            jnp.sum(conv_grad * padded[2:], axis=0),
            jnp.sum(conv_grad, axis=0),
        ]
    )
    conv_total = taken_together(conv_terms, FS) * scale
    whole_tokens = lax.all_gather(tokens, "tp", axis=0, tiled=True)
    full_gate, full_value = in_one_piece((up_gate_w, up_value_w), FS, 0, 1)
    joined = summed_rows(
        jnp.concatenate(
            [contract_rows(whole_tokens, gate_grad), contract_rows(whole_tokens, value_grad)],
            axis=1,
        ),
        FS,
    )
    gate_out = joined[:, :col_count] * scale
    value_out = joined[:, col_count:] * scale
    input_grad = summed_on_arrival(
        (contract_cols(gate_grad, full_gate) + contract_cols(value_grad, full_value)).astype(
            jnp.bfloat16
        ),
        "tp",
        0,
    ).astype(jnp.bfloat16)
    return (input_grad, gate_out, value_out, conv_total[:3], conv_total[3])


def solution(mesh):
    finer = Mesh(mesh.devices.reshape(8, 4, mesh.shape["tp"]), ("fs_0", "fs_1", "tp"))
    in_specs = (
        P(FS_TP, None),
        P(FS, "tp"),
        P(FS, "tp"),
        P(FS, "tp"),
        P(FS, "tp"),
        P(None, "tp"),
        P("tp"),
        P(FS, "tp"),
    )
    out_specs = (P(FS_TP, None), P(FS, "tp"), P(FS, "tp"), P(None, "tp"), P("tp"))
    return jax.shard_map(
        on_device, mesh=finer, in_specs=in_specs, out_specs=out_specs, check_vma=False
    )
```

profile of v0, /device:TPU:8, one launch (start us, length us, event | category | flops | bytes accessed | tf_op | source)
XLA Modules:
  0.0 301.7 jit_solution(17411305977214108581)
XLA Ops:
  7.2 0.0 copy-start
  7.2 0.0 copy-start.7
  7.2 0.0 copy-start.2
  7.2 0.0 copy-start.8
  7.2 0.0 all-gather.5.cloned.1.call-start
  7.3 0.7 all-gather.5.cloned.1.call-update
  7.9 0.0 all-gather.3.cloned.1.call-start
  8.0 1.8 pad_maximum_fusion.1
  9.8 0.0 all-gather.3.cloned.1.call-update
  9.8 0.0 reduce-scatter.5.cloned.1.call-start
  9.9 0.0 copy-start.3
  9.9 1.8 convert_element_type.26
  11.7 0.0 copy-done.7
  11.8 0.0 copy-done
  11.8 0.0 copy-done.2
  11.8 0.0 copy-done.8
  11.8 0.0 copy-done.3
  11.8 6.5 %multiply_reduce_fusion.2 = (f32[704]{0:T(1024)S(1)}, f32[704]{0:T(1024)S(1)}, f32[704]{0:T(1024)S(1)}, f32[704]{0:T(1024)S(1)}, f32[1024,704]{0,1:T(8,128)S(1)}, /*index=5*/f32[1024,704]{0,1:T(8,128)}) fusion(f32[1024,704]{0,1:T(8,128)S(1)} %convert_element_type.26, bf16[1024,704]{0,1:T(8,128)(2,1)S(1)} %copy-done, bf16[1024,704]{0,1:T(8,128)(2,1)S(1)} %copy-done.2, ...), kind=kLoop, calls=%fused_computation.29 | loop fusion | flops 25949440 | bytes 12998656 | tf_op jit(solution)/shard_map/reduce_sum | solution.py:87
  18.3 3.0 %fusion.6 = bf16[1024,704]{0,1:T(8,128)(2,1)} fusion(f32[1024,704]{0,1:T(8,128)S(1)} %get-tuple-element.32, f32[704]{0:T(1024)S(1)} %get-tuple-element.30, f32[704]{0:T(1024)S(1)} %get-tuple-element.31, f32[704]{0:T(1024)S(1)} %get-tuple-element.29), kind=kLoop, calls=%fused_computation.18 | loop fusion | flops 4325376 | bytes 4333824 | tf_op jit(solution)/shard_map/convert_element_type | solution.py:84
  21.4 0.0 copy-start.1
  21.4 25.0 %all-gather.5.cloned.1.call-done = bf16[1024,2048]{1,0:T(8,128)(2,1)} async-done(((bf16[128,2048]{1,0:T(8,128)(2,1)}), bf16[1024,2048]{1,0:T(8,128)(2,1)}) %all-gather.5.cloned.1.call-update) | async-done | bytes 4194320 | tf_op jit(solution)/shard_map/all_gather | solution.py:94
  46.4 0.0 copy-start.4
  46.4 0.0 copy-start.10
  46.4 8.4 %convolution_bitcast_fusion.1 = f32[2048,704]{0,1:T(8,128)} fusion(bf16[1024,704]{0,1:T(8,128)(2,1)} %fusion.6, bf16[1024,2048]{1,0:T(8,128)(2,1)} %all-gather.5.cloned.1.call-done), kind=kOutput, calls=%fused_computation.5 | convolution fusion | flops 2952790016 | bytes 11403264 | tf_op jit(solution)/shard_map/dot_general | solution.py:50
  54.8 0.0 copy-done.1
  54.8 0.0 copy-done.4
  54.8 0.0 copy-done.10
  54.8 5.3 %convolution_bitcast_fusion = f32[2048,704]{0,1:T(8,128)} fusion(bf16[1024,2048]{1,0:T(8,128)(2,1)S(1)} %copy-done.10, bf16[1024,704]{0,1:T(8,128)(2,1)S(1)} %copy-done.4, f32[1024,704]{0,1:T(8,128)S(1)} %copy-done.1), kind=kOutput, calls=%fused_computation.4 | convolution fusion | flops 2960719872 | bytes 14286848 | tf_op jit(solution)/shard_map/dot_general | solution.py:50
  60.1 10.8 %pad_maximum_fusion = f32[2048,1408]{0,1:T(8,128)} fusion(f32[2048,704]{0,1:T(8,128)} %convolution_bitcast_fusion, f32[2048,704]{0,1:T(8,128)} %convolution_bitcast_fusion.1), kind=kLoop, calls=%fused_computation | loop fusion | flops 2883584 | bytes 23068672 | tf_op jit(solution)/shard_map/concatenate | solution.py:97
  70.9 0.0 reduce-scatter.5.cloned.1.call-update
  71.0 0.8 broadcast_in_dim.2
  71.8 10.0 %all-to-all-start.1 = ((f32[32,4,704]{2,1,0:T(4,128)}), f32[32,4,704]{2,1,0:T(4,128)S(1)}, u32[]{:S(2)}, u32[]{:S(2)}) async-start(f32[32,4,704]{2,1,0:T(4,128)} %broadcast_in_dim.2), calls=%async_computation.2 | async-start | bytes 786432 | tf_op jit(solution)/shard_map/all_to_all | solution.py:13
  81.8 56.8 %all-gather.3.cloned.1.call-done = bf16[2048,1408]{1,0:T(8,128)(2,1)} async-done(((bf16[64,1408]{1,0:T(8,128)(2,1)}), bf16[2048,1408]{1,0:T(8,128)(2,1)}) %all-gather.3.cloned.1.call-update) | async-done | bytes 5767184 | tf_op jit(solution)/shard_map/all_gather | solution.py:28
  138.7 0.0 copy-start.5
  138.7 0.0 copy-start.9
  138.7 6.0 %fusion.1 = f32[1024,2048]{1,0:T(8,128)S(1)} fusion(bf16[1024,704]{0,1:T(8,128)(2,1)} %fusion.6, bf16[2048,1408]{1,0:T(8,128)(2,1)} %all-gather.3.cloned.1.call-done), kind=kOutput, calls=%fused_computation.13 | convolution fusion | flops 2952790016 | bytes 12976128 | tf_op jit(solution)/shard_map/dot_general | solution.py:56
  144.7 0.0 copy-done.5
  144.7 0.0 copy-done.9
  144.7 7.6 %add_convert_fusion = bf16[1024,2048]{1,0:T(8,128)(2,1)} fusion(f32[1024,2048]{1,0:T(8,128)S(1)} %fusion.1, bf16[2048,1408]{1,0:T(8,128)(2,1)S(1)} %copy-done.9, bf16[1024,704]{0,1:T(8,128)(2,1)S(1)} %copy-done.5, f32[1024,704]{0,1:T(8,128)S(1)} %copy-done.1), kind=kOutput, calls=%fused_computation.1 | convolution fusion | flops 2964914176 | bytes 20054016 | tf_op jit(solution)/shard_map/dot_general | solution.py:56
  152.3 0.0 all-to-all-done.1
  152.3 5.0 %all-to-all-start = ((bf16[8,128,2048]{2,1,0:T(8,128)(2,1)}), bf16[8,128,2048]{2,1,0:T(8,128)(2,1)}, u32[]{:S(2)}, u32[]{:S(2)}) async-start(bf16[8,128,2048]{2,1,0:T(8,128)(2,1)} %bitcast.11), calls=%async_computation | async-start | bytes 8388608 | tf_op jit(solution)/shard_map/all_to_all | solution.py:45
  157.3 0.0 reduce-scatter.7.cloned.1.call-start
  157.3 105.4 %reduce-scatter.5.cloned.1.call-done = f32[256,1408]{0,1:T(8,128)} async-done(((f32[2048,1408]{0,1:T(8,128)}), f32[256,1408]{0,1:T(8,128)}) %reduce-scatter.5.cloned.1.call-update) | async-done | bytes 1441808 | tf_op jit(solution)/shard_map/reduce_scatter | solution.py:33
  262.6 2.9 copy.22
  265.5 0.0 reduce-scatter.7.cloned.1.call-update
  265.6 0.1 reduce_sum.62
  265.7 0.0 copy-start.6
  265.7 0.6 slice_reduce_fusion
  266.3 0.0 all-to-all-done
  266.3 3.8 %reduce_sum.57 = bf16[128,2048]{1,0:T(8,128)(2,1)} reduce(bf16[8,128,2048]{2,1,0:T(8,128)(2,1)} %all-to-all-done, bf16[]{:T(256)} %constant.19.clone.1), dimensions={0}, to_apply=%region_0.1 | reduce | flops 1835008 | bytes 4718594 | tf_op jit(solution)/shard_map/reduce_sum | solution.py:46
  270.1 21.8 %reduce-scatter.7.cloned.1.call-done = f32[64,1408]{1,0:T(8,128)} async-done(((f32[256,1408]{1,0:T(8,128)}), f32[64,1408]{1,0:T(8,128)}) %reduce-scatter.7.cloned.1.call-update) | async-done | bytes 360464
  292.0 1.1 fusion.18
  293.1 0.2 copy.25
  293.3 0.0 copy-done.6
  293.3 0.8 copy.20
  294.1 0.2 copy.26
  294.3 0.8 copy.21
  (9 shorter events, 0.1 us)
Async XLA Ops:
  7.2 4.6 %copy-start = (bf16[1024,704]{0,1:T(8,128)(2,1)S(1)}, bf16[1024,704]{0,1:T(8,128)(2,1)}, u32[]{:S(2)}) copy-start(bf16[1024,704]{0,1:T(8,128)(2,1)} %param.9) | copy-start | bytes 4325380
  7.2 4.5 %copy-start.7 = (f32[3,704]{1,0:T(4,128)S(1)}, f32[3,704]{1,0:T(4,128)}, u32[]{:S(2)}) copy-start(f32[3,704]{1,0:T(4,128)} %param.13) | copy-start | bytes 25348
  7.2 4.6 %copy-start.2 = (bf16[1024,704]{0,1:T(8,128)(2,1)S(1)}, bf16[1024,704]{0,1:T(8,128)(2,1)}, u32[]{:S(2)}) copy-start(bf16[1024,704]{0,1:T(8,128)(2,1)} %param.10) | copy-start | bytes 4325380
  7.2 4.6 %copy-start.8 = (f32[704]{0:T(1024)S(1)}, f32[704]{0:T(1024)}, u32[]{:S(2)}) copy-start(f32[704]{0:T(1024)} %param.14) | copy-start | bytes 8452
  7.2 39.2 %all-gather.5.cloned.1.call-start = ((), (), s32[]{:S(2)}) async-start(), calls=%async_computation.5 | async-start | bytes 4718592 | tf_op jit(solution)/shard_map/all_gather | solution.py:94
  7.9 130.7 %all-gather.3.cloned.1.call-start = ((), (), s32[]{:S(2)}) async-start(), calls=%async_computation.4 | async-start | bytes 5947392 | tf_op jit(solution)/shard_map/all_gather | solution.py:28
  9.8 252.8 %reduce-scatter.5.cloned.1.call-start = ((), (), s32[]{:S(2)}) async-start(), calls=%async_computation.6 | async-start | bytes 12976128 | tf_op jit(solution)/shard_map/reduce_scatter | solution.py:33
  9.9 1.9 copy-start.3
  21.4 33.4 %copy-start.1 = (f32[1024,704]{0,1:T(8,128)S(1)}, f32[1024,704]{0,1:T(8,128)}, u32[]{:S(2)}) copy-start(f32[1024,704]{0,1:T(8,128)} %get-tuple-element.33) | copy-start | bytes 8650756
  46.4 8.4 %copy-start.4 = (bf16[1024,704]{0,1:T(8,128)(2,1)S(1)}, bf16[1024,704]{0,1:T(8,128)(2,1)}, u32[]{:S(2)}) copy-start(bf16[1024,704]{0,1:T(8,128)(2,1)} %param.15) | copy-start | bytes 4325380
  46.4 8.4 %copy-start.10 = (bf16[1024,2048]{1,0:T(8,128)(2,1)S(1)}, bf16[1024,2048]{1,0:T(8,128)(2,1)}, u32[]{:S(2)}) copy-start(bf16[1024,2048]{1,0:T(8,128)(2,1)} %all-gather.5.cloned.1.call-done) | copy-start | bytes 12582916
  71.8 80.4 %all-to-all-start.1 = ((f32[32,4,704]{2,1,0:T(4,128)}), f32[32,4,704]{2,1,0:T(4,128)S(1)}, u32[]{:S(2)}, u32[]{:S(2)}) async-start(f32[32,4,704]{2,1,0:T(4,128)} %broadcast_in_dim.2), calls=%async_computation.2 | async-start | bytes 786432 | tf_op jit(solution)/shard_map/all_to_all | solution.py:13
  138.7 6.0 %copy-start.5 = (bf16[1024,704]{0,1:T(8,128)(2,1)S(1)}, bf16[1024,704]{0,1:T(8,128)(2,1)}, u32[]{:S(2)}) copy-start(bf16[1024,704]{0,1:T(8,128)(2,1)} %param.15) | copy-start | bytes 4325380
  138.7 6.0 %copy-start.9 = (bf16[2048,1408]{1,0:T(8,128)(2,1)S(1)}, bf16[2048,1408]{1,0:T(8,128)(2,1)}, u32[]{:S(2)}) copy-start(bf16[2048,1408]{1,0:T(8,128)(2,1)} %all-gather.3.cloned.1.call-done) | copy-start | bytes 17301508
  152.3 114.0 %all-to-all-start = ((bf16[8,128,2048]{2,1,0:T(8,128)(2,1)}), bf16[8,128,2048]{2,1,0:T(8,128)(2,1)}, u32[]{:S(2)}, u32[]{:S(2)}) async-start(bf16[8,128,2048]{2,1,0:T(8,128)(2,1)} %bitcast.11), calls=%async_computation | async-start | bytes 8388608 | tf_op jit(solution)/shard_map/all_to_all | solution.py:45
  157.3 134.7 %reduce-scatter.7.cloned.1.call-start = ((), (), s32[]{:S(2)}) async-start(), calls=%async_computation.7 | async-start | bytes 1802240
  265.7 27.6 %copy-start.6 = (f32[4,704]{1,0:T(4,128)}, f32[4,704]{1,0:T(4,128)S(1)}, u32[]{:S(2)}) copy-start(f32[4,704]{1,0:T(4,128)S(1)} %broadcast_multiply_fusion.2) | copy-start | bytes 33796
Sparse Core Ops, SparseCore 0:
  9.9 36.4 all-gather.4
  49.5 89.0 all-gather.2
  141.2 121.3 reduce-scatter.4
  265.7 26.2 reduce-scatter.6
where the time goes:
time: 302 us
  waiting for transfers between devices  210 us (70%)
  other arithmetic  28 us (9%)
  matrix products  27.3 us (9%)
  starting transfers between devices  15.1 us (5%)
  between operations  14 us (5%)
  local copies, waits for them, and re-layouts  7.54 us (2%)
    reduce_scatter x1, waiting for transfers between devices, summed_rows(): subtotal = lax.psum_scatter(subtotal, axis, scatter_dimension=0, tiled=True)  105 us
    all_gather x1, waiting for transfers between devices, in_one_piece(): lax.all_gather(both, axis, axis=dim, tiled=True)  56.8 us
    all_gather x1, waiting for transfers between devices, on_device(): whole_tokens = lax.all_gather(tokens, 'tp', axis=0, tiled=True)  25 us
    unnamed x5, waiting for transfers between devices  22.5 us
    dot_general x2, matrix products, contract_rows(): lax.dot_general(left, right, (((0,), (0,)), ((), ())), preferred_element_...  13.7 us
    dot_general x2, matrix products, contract_cols(): lax.dot_general(left, right, (((1,), (1,)), ((), ())), preferred_element_...  13.6 us
    concatenate x1, other arithmetic, on_device(): jnp.concatenate([contract_rows(whole_tokens, gate_grad), contract_rows(wh...  10.8 us
    all_to_all x1, starting transfers between devices, copy_for_each(): lax.all_to_all(jnp.broadcast_to(shard[None], (peers, *shard.shape)), axis...  10 us
  transfers between devices with their start and end apart: 6, of which 4 were waited for; matrix products, arithmetic and copies ran while one was open for 20% of the time, Pallas kernels for 0%

commit v1 on v0

--- a/solution.py
+++ b/solution.py
@@ -91,7 +91,9 @@
         ]
     )
     conv_total = taken_together(conv_terms, FS) * scale
-    whole_tokens = lax.all_gather(tokens, "tp", axis=0, tiled=True)
+    whole_tokens = jnp.concatenate(
+        lax.all_to_all(jnp.stack([tokens] * lax.axis_size("tp")), "tp", 0, 0), axis=0
+    )
     full_gate, full_value = in_one_piece((up_gate_w, up_value_w), FS, 0, 1)
     joined = summed_rows(
         jnp.concatenate(

time: 302 us -> 267 us (0.88)
  waiting for transfers between devices: 210 us -> 158 us
  starting transfers between devices: 15.1 us -> 23 us
  local copies, waits for them, and re-layouts: 7.54 us -> 12.4 us
  matrix products: 27.3 us -> 30.5 us
    all_gather x1, waiting for transfers between devices: 56.8 us -> 0.02 us  [in_one_piece(): lax.all_gather(both, axis, axis=dim, tiled=True)]
    all_to_all x0 -> x1, waiting for transfers between devices: none -> 36.9 us  [on_device(): lax.all_to_all(jnp.stack([tokens] * lax.axis_size('tp')), 'tp', 0, 0)]
    all_gather x1 -> x0, waiting for transfers between devices: 25 us -> none  [on_device(): whole_tokens = lax.all_gather(tokens, 'tp', axis=0, tiled=True)]
    reduce_scatter x1, waiting for transfers between devices: 105 us -> 95.6 us  [summed_rows(): subtotal = lax.psum_scatter(subtotal, axis, scatter_dimension=0, tiled=True)]
    all_to_all x0 -> x1, starting transfers between devices: none -> 6.71 us  [on_device(): lax.all_to_all(jnp.stack([tokens] * lax.axis_size('tp')), 'tp', 0, 0)]
    all_to_all x1, waiting for transfers between devices: 0.01 us -> 4.28 us  [copy_for_each(): lax.all_to_all(jnp.broadcast_to(shard[None], (peers, *shard.shape)), axis...]
    another operation x0 -> x1, local copies, waits for them, and re-layouts: none -> 3.54 us  [on_device(): jnp.stack([tokens] * lax.axis_size('tp'))]
    unnamed x5 -> x4, waiting for transfers between devices: 22.5 us -> 21 us
  transfers between devices with their start and end apart: 6 -> 6, of which waited for: 4 -> 4; matrix products, arithmetic and copies ran while one was open for 20% -> 24% of each run, Pallas kernels for 0% -> 0%
where the time goes in v1:
time: 267 us; the launch traced here: 266 us
  waiting for transfers between devices  158 us (59%)
  matrix products  30.5 us (11%)
  other arithmetic  26.4 us (10%)
  starting transfers between devices  23 us (9%)
  between operations  15.7 us (6%)
  local copies, waits for them, and re-layouts  12.4 us (5%)
    reduce_scatter x1, waiting for transfers between devices, summed_rows(): subtotal = lax.psum_scatter(subtotal, axis, scatter_dimension=0, tiled=True)  95.6 us
    all_to_all x1, waiting for transfers between devices, on_device(): lax.all_to_all(jnp.stack([tokens] * lax.axis_size('tp')), 'tp', 0, 0)  36.9 us
    unnamed x4, waiting for transfers between devices  21 us
    dot_general x2, matrix products, contract_rows(): lax.dot_general(left, right, (((0,), (0,)), ((), ())), preferred_element_...  16 us
    dot_general x2, matrix products, contract_cols(): lax.dot_general(left, right, (((1,), (1,)), ((), ())), preferred_element_...  14.6 us
    concatenate x1, other arithmetic, on_device(): jnp.concatenate([contract_rows(whole_tokens, gate_grad), contract_rows(wh...  10.8 us
    all_to_all x1, starting transfers between devices, copy_for_each(): lax.all_to_all(jnp.broadcast_to(shard[None], (peers, *shard.shape)), axis...  9.75 us
    all_to_all x1, starting transfers between devices, on_device(): lax.all_to_all(jnp.stack([tokens] * lax.axis_size('tp')), 'tp', 0, 0)  6.71 us
  transfers between devices with their start and end apart: 6, of which 4 were waited for; matrix products, arithmetic and copies ran while one was open for 24% of the time, Pallas kernels for 0%

profile of v1, /device:TPU:8, one launch (start us, length us, event | category | flops | bytes accessed | tf_op | source)
XLA Modules:
  0.0 266.0 jit_solution(5725598318120674281)
XLA Ops:
  8.0 0.0 all-gather.2.cloned.1.call-start
  8.0 1.7 pad_maximum_fusion.1
  9.8 0.0 all-gather.2.cloned.1.call-update
  9.8 3.5 %stack.12 = bf16[8,128,2048]{2,1,0:T(8,128)(2,1)} broadcast(bf16[128,2048]{1,0:T(8,128)(2,1)} %param.8), dimensions={1,2} | broadcast | bytes 4718592 | tf_op jit(solution)/shard_map/stack | solution.py:95
  13.3 0.0 copy-start
  13.3 6.7 %all-to-all-start.1 = ((bf16[8,128,2048]{2,1,0:T(8,128)(2,1)}), bf16[8,128,2048]{2,1,0:T(8,128)(2,1)}, u32[]{:S(2)}, u32[]{:S(2)}) async-start(bf16[8,128,2048]{2,1,0:T(8,128)(2,1)} %stack.12), calls=%async_computation.1 | async-start | bytes 8388608 | tf_op jit(solution)/shard_map/all_to_all | solution.py:95
  20.0 0.0 copy-start.7
  20.0 0.0 copy-start.2
  20.0 0.0 copy-start.8
  20.0 0.0 reduce-scatter.5.cloned.1.call-start
  20.1 0.0 copy-done
  20.1 0.0 copy-start.3
  20.1 0.4 convert_element_type.26
  20.5 0.2 copy-done.7
  20.8 0.6 copy-done.2
  21.4 0.0 copy-done.8
  21.4 0.5 copy-done.3
  21.9 6.5 %multiply_reduce_fusion.2 = (f32[704]{0:T(1024)S(1)}, f32[704]{0:T(1024)S(1)}, f32[704]{0:T(1024)S(1)}, f32[704]{0:T(1024)S(1)}, f32[1024,704]{0,1:T(8,128)S(1)}, /*index=5*/f32[1024,704]{0,1:T(8,128)}) fusion(f32[1024,704]{0,1:T(8,128)S(1)} %convert_element_type.26, bf16[1024,704]{0,1:T(8,128)(2,1)S(1)} %copy-done, bf16[1024,704]{0,1:T(8,128)(2,1)S(1)} %copy-done.2, ...), kind=kLoop, calls=%fused_computation.29 | loop fusion | flops 25949440 | bytes 12998656 | tf_op jit(solution)/shard_map/reduce_sum | solution.py:87
  28.4 3.0 %fusion.6 = bf16[1024,704]{0,1:T(8,128)(2,1)} fusion(f32[1024,704]{0,1:T(8,128)S(1)} %get-tuple-element.32, f32[704]{0:T(1024)S(1)} %get-tuple-element.30, f32[704]{0:T(1024)S(1)} %get-tuple-element.31, f32[704]{0:T(1024)S(1)} %get-tuple-element.29), kind=kLoop, calls=%fused_computation.18 | loop fusion | flops 4325376 | bytes 4333824 | tf_op jit(solution)/shard_map/convert_element_type | solution.py:84
  31.4 36.9 %all-to-all-done.1 = bf16[8,128,2048]{2,1,0:T(8,128)(2,1)} async-done(((bf16[8,128,2048]{2,1,0:T(8,128)(2,1)}), bf16[8,128,2048]{2,1,0:T(8,128)(2,1)}, u32[]{:S(2)}, u32[]{:S(2)}) %all-to-all-start.1) | async-done | bytes 4194336 | tf_op jit(solution)/shard_map/all_to_all | solution.py:95
  68.4 0.0 copy-start.1
  68.4 0.0 copy-start.4
  68.4 8.4 %convolution_bitcast_fusion.1 = f32[2048,704]{0,1:T(8,128)} fusion(bf16[1024,704]{0,1:T(8,128)(2,1)} %fusion.6, bf16[1024,2048]{1,0:T(8,128)(2,1)} %bitcast.1), kind=kOutput, calls=%fused_computation.5 | convolution fusion | flops 2952790016 | bytes 11403264 | tf_op jit(solution)/shard_map/dot_general | solution.py:50
  76.8 0.0 copy-done.1
  76.8 0.0 copy-done.4
  76.8 7.5 %convolution_bitcast_fusion = f32[2048,704]{0,1:T(8,128)} fusion(bf16[1024,2048]{1,0:T(8,128)(2,1)} %bitcast.1, bf16[1024,704]{0,1:T(8,128)(2,1)S(1)} %copy-done.4, f32[1024,704]{0,1:T(8,128)S(1)} %copy-done.1), kind=kOutput, calls=%fused_computation.4 | convolution fusion | flops 2960719872 | bytes 14286848 | tf_op jit(solution)/shard_map/dot_general | solution.py:50
  84.3 10.8 %pad_maximum_fusion = f32[2048,1408]{0,1:T(8,128)} fusion(f32[2048,704]{0,1:T(8,128)} %convolution_bitcast_fusion, f32[2048,704]{0,1:T(8,128)} %convolution_bitcast_fusion.1), kind=kLoop, calls=%fused_computation | loop fusion | flops 2883584 | bytes 23068672 | tf_op jit(solution)/shard_map/concatenate | solution.py:99
  95.1 0.0 reduce-scatter.5.cloned.1.call-update
  95.2 0.8 broadcast_in_dim.2
  96.0 9.8 %all-to-all-start.2 = ((f32[32,4,704]{2,1,0:T(4,128)}), f32[32,4,704]{2,1,0:T(4,128)S(1)}, u32[]{:S(2)}, u32[]{:S(2)}) async-start(f32[32,4,704]{2,1,0:T(4,128)} %broadcast_in_dim.2), calls=%async_computation.3 | async-start | bytes 786432 | tf_op jit(solution)/shard_map/all_to_all | solution.py:13
  105.8 0.0 all-gather.2.cloned.1.call-done
  105.8 0.0 copy-start.5
  105.8 0.0 copy-start.9
  105.8 7.0 %fusion.1 = f32[1024,2048]{1,0:T(8,128)S(1)} fusion(bf16[1024,704]{0,1:T(8,128)(2,1)} %fusion.6, bf16[2048,1408]{1,0:T(8,128)(2,1)} %all-gather.2.cloned.1.call-done), kind=kOutput, calls=%fused_computation.13 | convolution fusion | flops 2952790016 | bytes 12976128 | tf_op jit(solution)/shard_map/dot_general | solution.py:56
  112.8 0.0 copy-done.5
  112.8 0.0 copy-done.9
  112.8 7.6 %add_convert_fusion = bf16[1024,2048]{1,0:T(8,128)(2,1)} fusion(f32[1024,2048]{1,0:T(8,128)S(1)} %fusion.1, bf16[2048,1408]{1,0:T(8,128)(2,1)S(1)} %copy-done.9, bf16[1024,704]{0,1:T(8,128)(2,1)S(1)} %copy-done.5, f32[1024,704]{0,1:T(8,128)S(1)} %copy-done.1), kind=kOutput, calls=%fused_computation.1 | convolution fusion | flops 2964914176 | bytes 20054016 | tf_op jit(solution)/shard_map/dot_general | solution.py:56
  120.4 4.3 %all-to-all-done.2 = f32[32,4,704]{2,1,0:T(4,128)S(1)} async-done(((f32[32,4,704]{2,1,0:T(4,128)}), f32[32,4,704]{2,1,0:T(4,128)S(1)}, u32[]{:S(2)}, u32[]{:S(2)}) %all-to-all-start.2) | async-done | bytes 360480 | tf_op jit(solution)/shard_map/all_to_all | solution.py:13
  124.7 6.5 %all-to-all-start = ((bf16[8,128,2048]{2,1,0:T(8,128)(2,1)}), bf16[8,128,2048]{2,1,0:T(8,128)(2,1)}, u32[]{:S(2)}, u32[]{:S(2)}) async-start(bf16[8,128,2048]{2,1,0:T(8,128)(2,1)} %bitcast.12), calls=%async_computation | async-start | bytes 8388608 | tf_op jit(solution)/shard_map/all_to_all | solution.py:45
  131.2 0.0 reduce-scatter.7.cloned.1.call-start
  131.2 95.6 %reduce-scatter.5.cloned.1.call-done = f32[256,1408]{0,1:T(8,128)} async-done(((f32[2048,1408]{0,1:T(8,128)}), f32[256,1408]{0,1:T(8,128)}) %reduce-scatter.5.cloned.1.call-update) | async-done | bytes 1441808 | tf_op jit(solution)/shard_map/reduce_scatter | solution.py:33
  226.8 2.9 %copy.22 = f32[256,1408]{1,0:T(8,128)} copy(f32[256,1408]{0,1:T(8,128)} %reduce-scatter.5.cloned.1.call-done) | data formatting | bytes 2883584
  229.8 0.0 reduce-scatter.7.cloned.1.call-update
  229.8 0.1 reduce_sum.62
  229.9 0.0 copy-start.6
  229.9 0.6 slice_reduce_fusion
  230.5 0.0 all-to-all-done
  230.5 3.8 %reduce_sum.57 = bf16[128,2048]{1,0:T(8,128)(2,1)} reduce(bf16[8,128,2048]{2,1,0:T(8,128)(2,1)} %all-to-all-done, bf16[]{:T(256)} %constant.19.clone.1), dimensions={0}, to_apply=%region_0.1 | reduce | flops 1835008 | bytes 4718594 | tf_op jit(solution)/shard_map/reduce_sum | solution.py:46
  234.3 21.0 %reduce-scatter.7.cloned.1.call-done = f32[64,1408]{1,0:T(8,128)} async-done(((f32[256,1408]{1,0:T(8,128)}), f32[64,1408]{1,0:T(8,128)}) %reduce-scatter.7.cloned.1.call-update) | async-done | bytes 360464
  255.3 1.1 fusion.18
  256.4 0.2 copy.25
  256.6 0.0 copy-done.6
  256.7 0.8 copy.20
  257.5 0.2 copy.26
  257.7 0.8 copy.21
  (9 shorter events, 0.1 us)
Async XLA Ops:
  8.0 97.8 %all-gather.2.cloned.1.call-start = ((), (), s32[]{:S(2)}) async-start(), calls=%async_computation.5 | async-start | bytes 5947392 | tf_op jit(solution)/shard_map/all_gather | solution.py:28
  13.3 6.8 %copy-start = (bf16[1024,704]{0,1:T(8,128)(2,1)S(1)}, bf16[1024,704]{0,1:T(8,128)(2,1)}, u32[]{:S(2)}) copy-start(bf16[1024,704]{0,1:T(8,128)(2,1)} %param.9) | copy-start | bytes 4325380
  13.3 55.0 %all-to-all-start.1 = ((bf16[8,128,2048]{2,1,0:T(8,128)(2,1)}), bf16[8,128,2048]{2,1,0:T(8,128)(2,1)}, u32[]{:S(2)}, u32[]{:S(2)}) async-start(bf16[8,128,2048]{2,1,0:T(8,128)(2,1)} %stack.12), calls=%async_computation.1 | async-start | bytes 8388608 | tf_op jit(solution)/shard_map/all_to_all | solution.py:95
  20.0 0.7 copy-start.7
  20.0 1.4 copy-start.2
  20.0 1.4 copy-start.8
  20.0 206.8 %reduce-scatter.5.cloned.1.call-start = ((), (), s32[]{:S(2)}) async-start(), calls=%async_computation.6 | async-start | bytes 12976128 | tf_op jit(solution)/shard_map/reduce_scatter | solution.py:33
  20.1 1.8 copy-start.3
  68.4 8.4 %copy-start.1 = (f32[1024,704]{0,1:T(8,128)S(1)}, f32[1024,704]{0,1:T(8,128)}, u32[]{:S(2)}) copy-start(f32[1024,704]{0,1:T(8,128)} %get-tuple-element.33) | copy-start | bytes 8650756
  68.4 8.4 %copy-start.4 = (bf16[1024,704]{0,1:T(8,128)(2,1)S(1)}, bf16[1024,704]{0,1:T(8,128)(2,1)}, u32[]{:S(2)}) copy-start(bf16[1024,704]{0,1:T(8,128)(2,1)} %param.15) | copy-start | bytes 4325380
  96.0 28.7 %all-to-all-start.2 = ((f32[32,4,704]{2,1,0:T(4,128)}), f32[32,4,704]{2,1,0:T(4,128)S(1)}, u32[]{:S(2)}, u32[]{:S(2)}) async-start(f32[32,4,704]{2,1,0:T(4,128)} %broadcast_in_dim.2), calls=%async_computation.3 | async-start | bytes 786432 | tf_op jit(solution)/shard_map/all_to_all | solution.py:13
  105.8 7.0 %copy-start.5 = (bf16[1024,704]{0,1:T(8,128)(2,1)S(1)}, bf16[1024,704]{0,1:T(8,128)(2,1)}, u32[]{:S(2)}) copy-start(bf16[1024,704]{0,1:T(8,128)(2,1)} %param.15) | copy-start | bytes 4325380
  105.8 7.0 %copy-start.9 = (bf16[2048,1408]{1,0:T(8,128)(2,1)S(1)}, bf16[2048,1408]{1,0:T(8,128)(2,1)}, u32[]{:S(2)}) copy-start(bf16[2048,1408]{1,0:T(8,128)(2,1)} %all-gather.2.cloned.1.call-done) | copy-start | bytes 17301508
  124.7 105.8 %all-to-all-start = ((bf16[8,128,2048]{2,1,0:T(8,128)(2,1)}), bf16[8,128,2048]{2,1,0:T(8,128)(2,1)}, u32[]{:S(2)}, u32[]{:S(2)}) async-start(bf16[8,128,2048]{2,1,0:T(8,128)(2,1)} %bitcast.12), calls=%async_computation | async-start | bytes 8388608 | tf_op jit(solution)/shard_map/all_to_all | solution.py:45
  131.2 124.1 %reduce-scatter.7.cloned.1.call-start = ((), (), s32[]{:S(2)}) async-start(), calls=%async_computation.7 | async-start | bytes 1802240
  229.9 26.8 %copy-start.6 = (f32[4,704]{1,0:T(4,128)}, f32[4,704]{1,0:T(4,128)S(1)}, u32[]{:S(2)}) copy-start(f32[4,704]{1,0:T(4,128)S(1)} %broadcast_multiply_fusion.2) | copy-start | bytes 33796
Sparse Core Ops, SparseCore 0:
  12.0 89.4 all-gather.1
Sparse Core Ops, SparseCore 1:
  95.2 131.5 reduce-scatter.4
  229.9 25.4 reduce-scatter.6
